TPU v7x, 32 devices: a whole 2x2x4 slice. The times are simulated.
32 devices in a mesh: sp: 32 (over z, y, x, core), tp: 1.
Axes of the slice: x: 2, y: 2, z: 4, core: 2. Of those that a mesh axis runs over, the one named last changes fastest.
Arguments:
- queries: bfloat16 [4096, 2048], P('sp', 'tp'), may hold values from -6 to 6
- forget_logits: bfloat16 [2, 4096, 2048], P(None, 'sp', 'tp'), may hold values from -7.5 to 7.5
- value_matrix: bfloat16 [4096, 2048], P('sp', 'tp'), may hold values from -6 to 6
- output_gate_logits: bfloat16 [4096, 2048], P('sp', 'tp'), may hold values from -6 to 6
- forget_slack: float32 [2048], P('tp'), may hold values from 0.00012207031 to 0.07
- spike_log_forget: float32 [4096, 16], P('sp', 'tp'), may hold values from -2.8 to 0, as said below
- head_norm_gain: bfloat16 [128], replicated, may hold values from 0.099609375 to 1.8984375
- output_weight: bfloat16 [2048, 2048], P('tp'), may hold values from -0.125 to 0.125
- residual: bfloat16 [4096, 2048], P('sp'), may hold values from -6 to 6
- mixer_norm_gain: bfloat16 [2048], replicated, may hold values from 0.099609375 to 1.8984375
- mixer_gate_weight: bfloat16 [2048, 5632], P('sp', 'tp'), may hold values from -0.125 to 0.125
- mixer_up_weight: bfloat16 [2048, 5632], P('sp', 'tp'), may hold values from -0.125 to 0.125
- mixer_down_weight: bfloat16 [5632, 2048], P('tp', 'sp'), may hold values from -0.078125 to 0.078125
Outputs:
- layer_out: bfloat16 [4096, 2048], P(('sp', 'tp'))
Inputs may be any that keep to these rules, and one draw needn't show every extreme that they name: `spike_log_forget`: zero at all but a few tokens.
All inputs are finite; a program needn't handle non-finite values.
Results may differ from a plain program's by a relative error of at most 0.015.
Values may be sent and summed in bfloat16 or wider, within the bound.
A program may use at most 192 MiB of HBM per device.

v0:
```python
import jax
import jax.numpy as jnp
from jax import lax
from jax.sharding import PartitionSpec as P

BLOCK = 128
NORM_EPS = 1e-06
BEST_PRECISION = lax.Precision.HIGHEST


def entering(array, axis, join, neutral, backward):
    count = lax.axis_size(axis)
    place = lax.axis_index(axis)
    ahead = count - 1 - place if backward else place
    gathered = jax.tree.map(
        lambda a, kind: lax.all_gather(a.astype(kind), axis), array, (jnp.bfloat16, jnp.bfloat16)
    )
    state = jax.tree.map(lambda a, e: jnp.zeros_like(a) + jnp.asarray(e, a.dtype), array, neutral)

    def one(turn, state):
        source = count - 1 - turn if backward else turn
        return join(
            state,
            jax.tree.map(
                lambda a, own: lax.dynamic_index_in_dim(a, source, 0, False).astype(own.dtype),
                gathered,
                array,
            ),
        )

    return lax.fori_loop(0, ahead, one, state)


def rms_scale(entries, gain_vec):
    return (
        entries
        * lax.rsqrt(jnp.mean(entries * entries, axis=-1, keepdims=True) + NORM_EPS)
        * gain_vec.astype(jnp.float32)
    )


def reverse_rows(tensor):
    return jnp.flip(tensor, 0)


def local_sweep(query_f, key_f, decay_f, value_f):
    row_count, heads_present, head_width = query_f.shape
    blocks_count = row_count // BLOCK
    tri_mask = jnp.tril(jnp.ones((BLOCK, BLOCK), bool))

    def to_blocks(tensor):
        return tensor.reshape(blocks_count, BLOCK, heads_present, head_width)

    def advance(carried, segment):
        state_now, offset = carried
        query_seg, key_seg, decay_seg, value_seg = segment
        running = jnp.cumsum(decay_seg, axis=0)
        query_scaled = query_seg * jnp.exp(running)
        key_scaled = key_seg * jnp.exp(-running)
        scores = jnp.einsum("thd,shd->hts", query_scaled, key_scaled, precision=BEST_PRECISION)
        scores = jnp.where(tri_mask[None], scores, 0.0)
        result = jnp.einsum("hts,shv->thv", scores, value_seg, precision=BEST_PRECISION)
        result = result + jnp.einsum(
            "thd,hdv->thv", query_scaled, state_now, precision=BEST_PRECISION
        )
        final_log = running[-1]
        state_next = jnp.exp(final_log)[:, :, None] * state_now + jnp.einsum(
            "shd,shv->hdv",
            key_seg * jnp.exp(final_log[None] - running),
            value_seg,
            precision=BEST_PRECISION,
        )
        reach = query_seg * jnp.exp(running + offset)
        return ((state_next, offset + final_log), (result, reach))

    initial = (
        jnp.zeros((heads_present, head_width, head_width), jnp.float32),
        jnp.zeros((heads_present, head_width), jnp.float32),
    )
    (state_end, offset_end), (results, reaches) = lax.scan(
        advance,
        initial,
        (to_blocks(query_f), to_blocks(key_f), to_blocks(decay_f), to_blocks(value_f)),
    )
    shape_back = (row_count, heads_present, head_width)
    return (
        results.reshape(shape_back),
        reaches.reshape(shape_back),
        state_end,
        jnp.exp(offset_end),
    )


def chain(earlier, latter):
    return (earlier[0] * latter[0], latter[0][..., None] * earlier[1] + latter[1])


def local(
    queries,
    forget_logits,
    value_matrix,
    output_gate_logits,
    forget_slack,
    spike_log_forget,
    head_norm_gain,
    output_weight,
    residual,
    mixer_norm_gain,
    mixer_gate_weight,
    mixer_up_weight,
    mixer_down_weight,
):
    row_count = queries.shape[0]
    heads_present = spike_log_forget.shape[1]
    head_width = queries.shape[1] // heads_present
    query_f = (jax.nn.silu(queries.astype(jnp.float32)) * head_width ** (-0.5)).reshape(
        row_count, heads_present, head_width
    )
    value_f = value_matrix.astype(jnp.float32).reshape(row_count, heads_present, head_width)
    gate_random_key = (forget_slack * jax.nn.sigmoid(-forget_logits.astype(jnp.float32))).reshape(
        2, row_count, heads_present, head_width
    )
    decay_logarithm = jnp.log1p(-gate_random_key) + spike_log_forget[None, :, :, None]
    fore_local, fore_reach, fore_state, fore_total = local_sweep(
        query_f, gate_random_key[0], decay_logarithm[0], value_f
    )
    back_local, back_reach, back_state, back_total = local_sweep(
        reverse_rows(query_f),
        reverse_rows(gate_random_key[1]),
        reverse_rows(decay_logarithm[1]),
        reverse_rows(value_f),
    )
    neutral = (jnp.ones_like(fore_total), jnp.zeros_like(fore_state))
    _, fore_enter = entering((fore_total, fore_state), "sp", chain, neutral, False)
    _, back_enter = entering((back_total, back_state), "sp", chain, neutral, True)
    fore_out = fore_local + jnp.einsum(
        "thd,hdv->thv", fore_reach, fore_enter, precision=BEST_PRECISION
    )
    back_out = back_local + jnp.einsum(
        "thd,hdv->thv", back_reach, back_enter, precision=BEST_PRECISION
    )
    mixture = fore_out + reverse_rows(back_out)
    mixed = (
        rms_scale(mixture, head_norm_gain).reshape(row_count, heads_present * head_width)
        * jax.nn.silu(output_gate_logits.astype(jnp.float32))
    ).astype(jnp.bfloat16)
    part_rows = row_count // lax.axis_size("tp")
    own_start = lax.axis_index("tp") * part_rows
    partial_out = jnp.dot(mixed, output_weight, preferred_element_type=jnp.float32).astype(
        jnp.bfloat16
    )
    mixer_add = lax.psum_scatter(
        lax.optimization_barrier(partial_out).astype(jnp.float32).astype(jnp.bfloat16),
        "tp",
        scatter_dimension=0,
        tiled=True,
    ).astype(jnp.float32)
    own_resid = lax.dynamic_slice_in_dim(residual, own_start, part_rows, 0)
    hidden_state = (own_resid.astype(jnp.float32) + mixer_add).astype(jnp.bfloat16)
    normed_part = rms_scale(hidden_state.astype(jnp.float32), mixer_norm_gain).astype(jnp.bfloat16)
    normed = lax.all_gather(normed_part, "tp", axis=0, tiled=True)
    gate_act = jnp.dot(
        normed,
        lax.all_gather(mixer_gate_weight, "sp", axis=0, tiled=True),
        preferred_element_type=jnp.float32,
    )
    up_act = jnp.dot(
        normed,
        lax.all_gather(mixer_up_weight, "sp", axis=0, tiled=True),
        preferred_element_type=jnp.float32,
    )
    inner = (jax.nn.silu(gate_act) * up_act).astype(jnp.bfloat16)
    lowered = jnp.dot(
        inner,
        lax.all_gather(mixer_down_weight, "sp", axis=1, tiled=True),
        preferred_element_type=jnp.float32,
    )
    lowered_term = lax.optimization_barrier(lowered.astype(jnp.bfloat16)).astype(jnp.float32)
    ffn_add = lax.psum_scatter(
        lowered_term.astype(jnp.bfloat16), "tp", scatter_dimension=0, tiled=True
    ).astype(jnp.float32)
    return (hidden_state.astype(jnp.float32) + ffn_add).astype(jnp.bfloat16)


def solution(mesh):
    placed = (
        P("sp", "tp"),
        P(None, "sp", "tp"),
        P("sp", "tp"),
        P("sp", "tp"),
        P("tp"),
        P("sp", "tp"),
        P(),
        P("tp", None),
        P("sp", None),
        P(),
        P("sp", "tp"),
        P("sp", "tp"),
        P("tp", "sp"),
    )
    return jax.shard_map(
        local, mesh=mesh, in_specs=placed, out_specs=P(("sp", "tp"), None), check_vma=False
    )
```

profile of v0, /device:TPU:0, one launch (start us, length us, event | category | flops | bytes accessed | tf_op | source)
XLA Modules:
  0.0 728.9 jit_solution(13368527805004820737)
XLA Ops:
  6.5 2.4 divide_multiply_fusion
  9.0 1.7 copy.55
  10.7 3.3 bitcast_add_fusion
  14.0 2.3 slice_bitcast_fusion.1
  16.3 2.3 rev.17
  18.5 2.4 fusion.49
  26.6 3.6 exponential_multiply_fusion
  30.2 3.0 fusion.7
  33.3 1.4 copy.56
  34.7 1.4 fusion.21
  36.1 2.8 bitcast_multiply_fusion
  38.9 2.1 fusion.6
  43.0 44.7 %all_gather.33 = bf16[32,16,128]{2,1,0:T(8,128)(2,1)S(1)} all-gather(bf16[1,16,128]{2,1,0:T(8,128)(2,1)S(1)} %get-tuple-element.230), channel_id=1, replica_groups=mesh['sp'=32,'tp'=1] {'sp'}, dimensions={0}, use_global_device_ids=true | all-gather | bytes 135168 | tf_op jit(solution)/shard_map/all_gather | solution.py:16
  87.7 39.0 %all_gather.30 = bf16[32,16,128]{2,1,0:T(8,128)(2,1)S(1)} all-gather(bf16[1,16,128]{2,1,0:T(8,128)(2,1)S(1)} %get-tuple-element.227), channel_id=1, replica_groups=mesh['sp'=32,'tp'=1] {'sp'}, dimensions={0}, use_global_device_ids=true | all-gather | bytes 135168 | tf_op jit(solution)/shard_map/all_gather | solution.py:16
  126.7 4.0 convolution_select_fusion.1
  130.8 1.2 convolution_bitcast_fusion.5
  132.0 2.8 convolution_select_fusion
  134.8 1.9 convolution_bitcast_fusion.2
  136.7 3.4 fusion.2
  140.1 3.4 fusion.5
  143.5 7.9 %all-gather.16.cloned.1.call-done = bf16[512,128,128]{2,1,0:T(8,128)(2,1)} async-done(((bf16[16,128,128]{2,1,0:T(8,128)(2,1)}), bf16[512,128,128]{2,1,0:T(8,128)(2,1)}) %all-gather.16.cloned.1.call-update) | async-done | bytes 16777232 | tf_op jit(solution)/shard_map/all_gather | solution.py:16
  151.5 49.8 %while.17 = (s32[]{:T(128)}, f32[16,128,128]{2,1,0:T(8,128)S(1)}, s32[]{:T(128)}, bf16[32,16,128]{2,1,0:T(8,128)(2,1)S(1)}, bf16[32,16,128,128]{3,2,1,0:T(8,128)...) while((s32[]{:T(128)}, f32[16,128,128]{2,1,0:T(8,128)S(1)}, s32[]{:T(128)}, ...), condition=%wide.region_5.6_spmd, body=%wide.region_4.5_spmd.sunk | while | flops 788486 | bytes 2642067 | solution.py:31
  151.6 1.5 convert_add_fusion.6
  153.1 1.5 convert_add_fusion.6
  154.7 1.5 convert_add_fusion.6
  156.3 1.5 convert_add_fusion.6
  157.9 1.5 convert_add_fusion.6
  159.5 1.5 convert_add_fusion.6
  161.1 1.6 convert_add_fusion.6
  162.7 1.5 convert_add_fusion.6
  164.3 1.5 convert_add_fusion.6
  165.9 1.5 convert_add_fusion.6
  167.5 1.5 convert_add_fusion.6
  169.1 1.6 convert_add_fusion.6
  170.7 1.5 convert_add_fusion.6
  172.3 1.5 convert_add_fusion.6
  173.9 1.5 convert_add_fusion.6
  175.5 1.5 convert_add_fusion.6
  177.1 1.5 convert_add_fusion.6
  178.7 1.5 convert_add_fusion.6
  180.3 1.5 convert_add_fusion.6
  181.9 1.7 convert_add_fusion.6
  183.6 1.5 convert_add_fusion.6
  185.2 1.5 convert_add_fusion.6
  186.8 1.5 convert_add_fusion.6
  188.4 1.5 convert_add_fusion.6
  190.0 1.5 convert_add_fusion.6
  191.6 1.5 convert_add_fusion.6
  193.2 1.5 convert_add_fusion.6
  194.8 1.5 convert_add_fusion.6
  196.4 1.5 convert_add_fusion.6
  198.0 1.5 convert_add_fusion.6
  199.6 1.5 convert_add_fusion.6
  201.3 4.7 fusion.1
  206.0 9.3 %rev.20 = f32[128,16,128]{0,2,1:T(8,128)} reverse(f32[128,16,128]{0,2,1:T(8,128)} %fusion.1), dimensions={0} | reverse | bytes 2097152 | tf_op jit(solution)/shard_map/jit(_flip)/rev | solution.py:43
  215.3 52.1 %all-gather.14.cloned.1.call-done = bf16[512,128,128]{2,1,0:T(8,128)(2,1)} async-done(((bf16[16,128,128]{2,1,0:T(8,128)(2,1)}), bf16[512,128,128]{2,1,0:T(8,128)(2,1)}) %all-gather.14.cloned.1.call-update) | async-done | bytes 16777232 | tf_op jit(solution)/shard_map/all_gather | solution.py:16
  267.6 1.2 copy-done.4
  268.8 3.7 multiply_reduce_fusion
  273.5 5.0 convolution_convert_fusion
  278.9 133.5 %all-gather.8.cloned.1.call-done = bf16[2048,5632]{1,0:T(8,128)(2,1)} async-done(((bf16[64,5632]{1,0:T(8,128)(2,1)}), bf16[2048,5632]{1,0:T(8,128)(2,1)}) %all-gather.8.cloned.1.call-update) | async-done | bytes 23068688 | tf_op jit(solution)/shard_map/all_gather | solution.py:164
  412.4 12.4 %fusion.43 = f32[128,5632]{1,0:T(8,128)} fusion(bf16[2048,5632]{1,0:T(8,128)(2,1)} %all-gather.8.cloned.1.call-done, bf16[128,2048]{1,0:T(8,128)(2,1)S(1)} %get-tuple-element.216, f32[2048]{0:T(1024)S(1)} %convert_element_type.124, f32[128]{0:T(128)S(1)} %add_rsqrt_fusion.1), kind=kOutput, calls=%fused_computation.81 | convolution fusion | flops 2953838592 | bytes 26485248 | tf_op jit(solution)/shard_map/dot_general | solution.py:162
  424.9 132.3 %all-gather.10.cloned.1.call-done = bf16[2048,5632]{1,0:T(8,128)(2,1)} async-done(((bf16[64,5632]{1,0:T(8,128)(2,1)}), bf16[2048,5632]{1,0:T(8,128)(2,1)}) %all-gather.10.cloned.1.call-update) | async-done | bytes 23068688 | tf_op jit(solution)/shard_map/all_gather | solution.py:169
  557.2 144.8 %all-gather.12.cloned.1.call-done = bf16[5632,2048]{0,1:T(8,128)(2,1)} async-done(((bf16[5632,64]{0,1:T(8,128)(2,1)}), bf16[5632,2048]{0,1:T(8,128)(2,1)}) %all-gather.12.cloned.1.call-update) | async-done | bytes 23068688 | tf_op jit(solution)/shard_map/all_gather | solution.py:175
  702.0 19.5 %convolution_convert_fusion.1 = bf16[128,2048]{1,0:T(8,128)(2,1)S(1)} fusion(bf16[5632,2048]{0,1:T(8,128)(2,1)} %all-gather.12.cloned.1.call-done, bf16[2048,5632]{1,0:T(8,128)(2,1)} %all-gather.10.cloned.1.call-done, f32[128,5632]{1,0:T(8,128)} %fusion.43, bf16[128,2048]{1,0:T(8,128)(2,1)S(1)} %get-tuple-element.216, f32[2048]{0:T(1024)S(1)} %convert_element_type.124, ...), kind=kOutput, calls=%fused_computation.7 | convolution fusion | flops 5911216128 | bytes 50078208 | tf_op jit(solution)/shard_map/dot_general | solution.py:173
  (87 shorter events, 10.5 us)
Async XLA Ops:
  6.5 19.5 %copy-start = (bf16[128,2048]{1,0:T(8,128)(2,1)S(1)}, bf16[128,2048]{1,0:T(8,128)(2,1)}, u32[]{:S(2)}) copy-start(bf16[128,2048]{1,0:T(8,128)(2,1)} %param.19) | copy-start | bytes 1572868
  6.5 144.9 %all-gather.16.cloned.1.call-start = ((), (), s32[]{:S(2)}) async-start(), calls=%async_computation.4 | async-start | bytes 17301504 | tf_op jit(solution)/shard_map/all_gather | solution.py:16
  8.9 1.7 copy-start.8
  22.3 2.3 copy-start.6
  26.6 3.7 copy-start.2
  33.3 234.2 %all-gather.14.cloned.1.call-start = ((), (), s32[]{:S(2)}) async-start(), calls=%async_computation.3 | async-start | bytes 17301504 | tf_op jit(solution)/shard_map/all_gather | solution.py:16
  38.9 4.1 copy-start.11
  38.9 4.1 copy-start.9
  41.1 371.3 %all-gather.8.cloned.1.call-start = ((), (), s32[]{:S(2)}) async-start(), calls=%async_computation | async-start | bytes 23789568 | tf_op jit(solution)/shard_map/all_gather | solution.py:164
  41.8 515.4 %all-gather.10.cloned.1.call-start = ((), (), s32[]{:S(2)}) async-start(), calls=%async_computation.1 | async-start | bytes 23789568 | tf_op jit(solution)/shard_map/all_gather | solution.py:169
  42.4 659.6 %all-gather.12.cloned.1.call-start = ((), (), s32[]{:S(2)}) async-start(), calls=%async_computation.2 | async-start | bytes 23789568 | tf_op jit(solution)/shard_map/all_gather | solution.py:175
  126.7 5.3 copy-start.5
  130.8 4.0 copy-start.3
  267.6 1.2 copy-start.4
  272.5 1.0 copy-start.10
  273.5 5.0 copy-start.7
  702.0 20.4 %copy-start.1 = (bf16[128,2048]{1,0:T(8,128)(2,1)S(1)}, bf16[128,2048]{1,0:T(8,128)(2,1)}, u32[]{:S(2)}) copy-start(bf16[128,2048]{1,0:T(8,128)(2,1)} %param.19) | copy-start | bytes 1572868
Sparse Core Ops, SparseCore 0:
  33.4 117.9 all-gather.15
  154.3 113.1 all-gather.13
  270.3 142.0 all-gather.7
  415.1 142.0 all-gather.9
  559.9 142.0 all-gather.11
where the time goes:
time: 732 us; the launch traced here: 729 us
  waiting for transfers between devices  472 us (64%)
  blocking collectives  83.7 us (11%)
  other arithmetic  67.5 us (9%)
  matrix products  67.2 us (9%)
  local copies, waits for them, and re-layouts  23.1 us (3%)
  between operations  13.4 us (2%)
    all_gather x1, waiting for transfers between devices, local(): lax.all_gather(mixer_down_weight, 'sp', axis=1, tiled=True)  145 us
    all_gather x1, waiting for transfers between devices, local(): lax.all_gather(mixer_gate_weight, 'sp', axis=0, tiled=True)  134 us
    all_gather x1, waiting for transfers between devices, local(): lax.all_gather(mixer_up_weight, 'sp', axis=0, tiled=True)  132 us
    all_gather x2, blocking collectives, entering(): lax.all_gather(a.astype(kind), axis)  83.7 us
    all_gather x2, waiting for transfers between devices, entering(): lax.all_gather(a.astype(kind), axis)  60 us
    add x31, other arithmetic, chain(): latter[0][..., None] * earlier[1] + latter[1]  48.1 us
    dot_general x1, matrix products, local(): jnp.dot(inner, lax.all_gather(mixer_down_weight, 'sp', axis=1, tiled=True...  19.5 us
  transfers between devices with their start and end apart: 5, of which 5 were waited for; matrix products, arithmetic and copies ran while one was open for 15% of the time, Pallas kernels for 0%

commit v1 on v0

--- a/solution.py
+++ b/solution.py
@@ -172,7 +172,7 @@
     inner = (jax.nn.silu(gate_act) * up_act).astype(jnp.bfloat16)
     lowered = jnp.dot(
         inner,
-        lax.all_gather(mixer_down_weight, "sp", axis=1, tiled=True),
+        jnp.concatenate(lax.all_gather(mixer_down_weight, "sp"), axis=1),
         preferred_element_type=jnp.float32,
     )
     lowered_term = lax.optimization_barrier(lowered.astype(jnp.bfloat16)).astype(jnp.float32)

time: 732 us -> 757 us (1.034)
  waiting for transfers between devices: 472 us -> 442 us
  local copies, waits for them, and re-layouts: 23.1 us -> 51.7 us
  other arithmetic: 67.5 us -> 86.9 us
    another operation x2, other arithmetic: 3.72 us -> 24.7 us  [advance(): running = jnp.cumsum(decay_seg, axis=0)]
    all_gather x1, waiting for transfers between devices: 134 us -> 114 us  [local(): lax.all_gather(mixer_gate_weight, 'sp', axis=0, tiled=True)]
    unnamed x30 -> x35, local copies, waits for them, and re-layouts: 8.36 us -> 27.1 us
    reshape x0 -> x1, local copies, waits for them, and re-layouts: none -> 14.3 us  [local(): jnp.concatenate(lax.all_gather(mixer_down_weight, 'sp'), axis=1)]
    all_gather x1, waiting for transfers between devices: 145 us -> 134 us  [local(): lax.all_gather(mixer_down_weight, 'sp')]
  transfers between devices with their start and end apart: 5 -> 5, of which waited for: 5 -> 5; matrix products, arithmetic and copies ran while one was open for 15% -> 19% of each run, Pallas kernels for 0% -> 0%
where the time goes in v1:
time: 757 us; the launch traced here: 747 us
  waiting for transfers between devices  442 us (58%)
  other arithmetic  86.9 us (11%)
  blocking collectives  84 us (11%)
  matrix products  67.6 us (9%)
  local copies, waits for them, and re-layouts  51.7 us (7%)
  between operations  13.7 us (2%)
    all_gather x1, waiting for transfers between devices, local(): lax.all_gather(mixer_down_weight, 'sp')  134 us
    all_gather x1, waiting for transfers between devices, local(): lax.all_gather(mixer_up_weight, 'sp', axis=0, tiled=True)  132 us
    all_gather x1, waiting for transfers between devices, local(): lax.all_gather(mixer_gate_weight, 'sp', axis=0, tiled=True)  114 us
    all_gather x2, blocking collectives, entering(): lax.all_gather(a.astype(kind), axis)  84 us
    all_gather x2, waiting for transfers between devices, entering(): lax.all_gather(a.astype(kind), axis)  59.6 us
    add x31, other arithmetic, chain(): latter[0][..., None] * earlier[1] + latter[1]  48 us
    unnamed x35, local copies, waits for them, and re-layouts  27.1 us
    another operation x2, other arithmetic, advance(): running = jnp.cumsum(decay_seg, axis=0)  24.7 us
  transfers between devices with their start and end apart: 5, of which 5 were waited for; matrix products, arithmetic and copies ran while one was open for 19% of the time, Pallas kernels for 0%

profile of v1, /device:TPU:0, one launch (start us, length us, event | category | flops | bytes accessed | tf_op | source)
XLA Modules:
  0.0 747.3 jit_solution(11760159474741531491)
XLA Ops:
  6.5 3.7 divide_multiply_fusion
  10.2 1.7 copy.95
  12.0 1.9 bitcast_add_fusion
  14.0 1.3 copy-done.5
  15.4 23.3 %fusion.49 = f32[128,16,128]{2,1,0:T(8,128)S(1)} fusion(f32[128,16,128]{2,1,0:T(8,128)S(1)} %rev.17), kind=kOutput, calls=%fused_computation.95 | output fusion | flops 33292288 | bytes 2097152 | tf_op jit(solution)/shard_map/while/body/eval_jaxpr/jit(cumsum)/reduce_window_sum | solution.py:57
  38.8 3.1 slice_bitcast_fusion.2
  45.0 3.6 exponential_multiply_fusion
  48.7 3.0 fusion.7
  51.7 1.4 copy.96
  53.2 1.4 fusion.21
  54.5 2.8 bitcast_multiply_fusion
  57.3 2.1 fusion.6
  61.5 44.7 %all_gather.36 = bf16[32,16,128]{2,1,0:T(8,128)(2,1)S(1)} all-gather(bf16[1,16,128]{2,1,0:T(8,128)(2,1)S(1)} %get-tuple-element.230), channel_id=1, replica_groups=mesh['sp'=32,'tp'=1] {'sp'}, dimensions={0}, use_global_device_ids=true | all-gather | bytes 135168 | tf_op jit(solution)/shard_map/all_gather | solution.py:16
  106.1 39.3 %all_gather.33 = bf16[32,16,128]{2,1,0:T(8,128)(2,1)S(1)} all-gather(bf16[1,16,128]{2,1,0:T(8,128)(2,1)S(1)} %get-tuple-element.227), channel_id=1, replica_groups=mesh['sp'=32,'tp'=1] {'sp'}, dimensions={0}, use_global_device_ids=true | all-gather | bytes 135168 | tf_op jit(solution)/shard_map/all_gather | solution.py:16
  145.5 4.0 convolution_select_fusion.1
  150.8 2.8 convolution_select_fusion
  153.5 1.9 convolution_bitcast_fusion.2
  155.4 3.4 fusion.2
  158.9 3.4 fusion.5
  162.3 7.9 %all-gather.15.cloned.1.call-done = bf16[512,128,128]{2,1,0:T(8,128)(2,1)} async-done(((bf16[16,128,128]{2,1,0:T(8,128)(2,1)}), bf16[512,128,128]{2,1,0:T(8,128)(2,1)}) %all-gather.15.cloned.1.call-update) | async-done | bytes 16777232 | tf_op jit(solution)/shard_map/all_gather | solution.py:16
  170.3 49.7 %while.17 = (s32[]{:T(128)}, f32[16,128,128]{2,1,0:T(8,128)S(1)}, s32[]{:T(128)}, bf16[32,16,128]{2,1,0:T(8,128)(2,1)S(1)}, bf16[32,16,128,128]{3,2,1,0:T(8,128)...) while((s32[]{:T(128)}, f32[16,128,128]{2,1,0:T(8,128)S(1)}, s32[]{:T(128)}, ...), condition=%wide.region_5.6_spmd, body=%wide.region_4.5_spmd.sunk | while | flops 788486 | bytes 2642067 | solution.py:31
  170.4 1.5 convert_add_fusion.6
  172.0 1.5 convert_add_fusion.6
  173.6 1.5 convert_add_fusion.6
  175.2 1.5 convert_add_fusion.6
  176.7 1.5 convert_add_fusion.6
  178.3 1.6 convert_add_fusion.6
  180.0 1.6 convert_add_fusion.6
  181.6 1.5 convert_add_fusion.6
  183.2 1.5 convert_add_fusion.6
  184.8 1.5 convert_add_fusion.6
  186.4 1.5 convert_add_fusion.6
  188.0 1.5 convert_add_fusion.6
  189.5 1.5 convert_add_fusion.6
  191.1 1.6 convert_add_fusion.6
  192.7 1.5 convert_add_fusion.6
  194.3 1.5 convert_add_fusion.6
  195.9 1.5 convert_add_fusion.6
  197.5 1.5 convert_add_fusion.6
  199.1 1.5 convert_add_fusion.6
  200.7 1.6 convert_add_fusion.6
  202.4 1.5 convert_add_fusion.6
  203.9 1.5 convert_add_fusion.6
  205.5 1.5 convert_add_fusion.6
  207.1 1.5 convert_add_fusion.6
  208.7 1.5 convert_add_fusion.6
  210.3 1.5 convert_add_fusion.6
  211.9 1.5 convert_add_fusion.6
  213.5 1.5 convert_add_fusion.6
  215.1 1.6 convert_add_fusion.6
  216.7 1.5 convert_add_fusion.6
  218.3 1.6 convert_add_fusion.6
  220.0 5.0 fusion.1
  225.0 9.3 %rev.20 = f32[128,16,128]{0,2,1:T(8,128)} reverse(f32[128,16,128]{0,2,1:T(8,128)} %fusion.1), dimensions={0} | reverse | bytes 2097152 | tf_op jit(solution)/shard_map/jit(_flip)/rev | solution.py:43
  234.3 51.6 %all-gather.13.cloned.1.call-done = bf16[512,128,128]{2,1,0:T(8,128)(2,1)} async-done(((bf16[16,128,128]{2,1,0:T(8,128)(2,1)}), bf16[512,128,128]{2,1,0:T(8,128)(2,1)}) %all-gather.13.cloned.1.call-update) | async-done | bytes 16777232 | tf_op jit(solution)/shard_map/all_gather | solution.py:16
  286.1 4.0 multiply_reduce_fusion
  291.1 4.8 convolution_convert_fusion
  296.2 134.3 %all-gather.17.cloned.1.call-done = bf16[180224,64]{0,1:T(8,128)(2,1)} async-done(((bf16[5632,64]{0,1:T(8,128)(2,1)}), bf16[180224,64]{0,1:T(8,128)(2,1)}) %all-gather.17.cloned.1.call-update) | async-done | bytes 23068688 | tf_op jit(solution)/shard_map/all_gather | solution.py:175
  430.5 16.6 %copy.98 = bf16[8,8,32,5632]{3,2,1,0:T(8,128)(2,1)S(1)} copy(bf16[8,8,32,5632]{3,1,2,0:T(8,128)(2,1)} %bitcast.112) | data formatting | bytes 46137344
  447.1 14.3 %copy.87 = bf16[5632,32,64]{0,2,1:T(8,128)(2,1)} copy(bf16[5632,32,64]{0,1,2:T(8,128)(2,1)S(1)} %bitcast.111) | data formatting | bytes 46137344 | tf_op jit(solution)/shard_map/reshape | solution.py:175
  461.4 113.9 %all-gather.9.cloned.1.call-done = bf16[2048,5632]{1,0:T(8,128)(2,1)} async-done(((bf16[64,5632]{1,0:T(8,128)(2,1)}), bf16[2048,5632]{1,0:T(8,128)(2,1)}) %all-gather.9.cloned.1.call-update) | async-done | bytes 23068688 | tf_op jit(solution)/shard_map/all_gather | solution.py:164
  575.3 12.4 %fusion.43 = f32[128,5632]{1,0:T(8,128)} fusion(bf16[2048,5632]{1,0:T(8,128)(2,1)} %all-gather.9.cloned.1.call-done, bf16[128,2048]{1,0:T(8,128)(2,1)S(1)} %get-tuple-element.216, f32[2048]{0:T(1024)S(1)} %convert_element_type.124, f32[128]{0:T(128)S(1)} %add_rsqrt_fusion.1), kind=kOutput, calls=%fused_computation.81 | convolution fusion | flops 2953838592 | bytes 26485248 | tf_op jit(solution)/shard_map/dot_general | solution.py:162
  587.8 132.3 %all-gather.11.cloned.1.call-done = bf16[2048,5632]{1,0:T(8,128)(2,1)} async-done(((bf16[64,5632]{1,0:T(8,128)(2,1)}), bf16[2048,5632]{1,0:T(8,128)(2,1)}) %all-gather.11.cloned.1.call-update) | async-done | bytes 23068688 | tf_op jit(solution)/shard_map/all_gather | solution.py:169
  720.1 19.5 %convolution_convert_fusion.1 = bf16[128,2048]{1,0:T(8,128)(2,1)S(1)} fusion(bf16[5632,2048]{0,1:T(8,128)(2,1)} %bitcast.113, bf16[2048,5632]{1,0:T(8,128)(2,1)} %all-gather.11.cloned.1.call-done, f32[128,5632]{1,0:T(8,128)} %fusion.43, bf16[128,2048]{1,0:T(8,128)(2,1)S(1)} %get-tuple-element.216, f32[2048]{0:T(1024)S(1)} %convert_element_type.124, ...), kind=kOutput, calls=%fused_computation.7 | convolution fusion | flops 5911216128 | bytes 50078208 | tf_op jit(solution)/shard_map/dot_general | solution.py:173
  (93 shorter events, 9.3 us)
Async XLA Ops:
  6.5 38.0 %copy-start = (bf16[128,2048]{1,0:T(8,128)(2,1)S(1)}, bf16[128,2048]{1,0:T(8,128)(2,1)}, u32[]{:S(2)}) copy-start(bf16[128,2048]{1,0:T(8,128)(2,1)} %param.19) | copy-start | bytes 1572868
  6.5 163.7 %all-gather.15.cloned.1.call-start = ((), (), s32[]{:S(2)}) async-start(), calls=%async_computation.3 | async-start | bytes 17301504 | tf_op jit(solution)/shard_map/all_gather | solution.py:16
  10.2 1.7 copy-start.10
  14.0 1.3 copy-start.5
  38.8 4.3 copy-start.6
  38.8 4.2 copy-start.8
  45.0 3.7 copy-start.3
  48.7 106.8 %copy-start.2 = (f32[128,16,128]{2,1,0:T(8,128)}, f32[128,16,128]{2,1,0:T(8,128)S(1)}, u32[]{:S(2)}) copy-start(f32[128,16,128]{2,1,0:T(8,128)S(1)} %get-tuple-element.228) | copy-start | bytes 3145732
  51.7 234.2 %all-gather.13.cloned.1.call-start = ((), (), s32[]{:S(2)}) async-start(), calls=%async_computation.2 | async-start | bytes 17301504 | tf_op jit(solution)/shard_map/all_gather | solution.py:16
  57.3 4.1 copy-start.13
  57.3 4.1 copy-start.11
  59.5 371.0 %all-gather.17.cloned.1.call-start = ((), (), s32[]{:S(2)}) async-start(), calls=%async_computation.4 | async-start | bytes 23789568 | tf_op jit(solution)/shard_map/all_gather | solution.py:175
  60.2 515.1 %all-gather.9.cloned.1.call-start = ((), (), s32[]{:S(2)}) async-start(), calls=%async_computation | async-start | bytes 23789568 | tf_op jit(solution)/shard_map/all_gather | solution.py:164
  60.8 659.3 %all-gather.11.cloned.1.call-start = ((), (), s32[]{:S(2)}) async-start(), calls=%async_computation.1 | async-start | bytes 23789568 | tf_op jit(solution)/shard_map/all_gather | solution.py:169
  145.5 5.3 copy-start.7
  149.5 4.0 copy-start.4
  290.1 1.0 copy-start.12
  291.1 4.8 copy-start.9
  720.1 20.4 %copy-start.1 = (bf16[128,2048]{1,0:T(8,128)(2,1)S(1)}, bf16[128,2048]{1,0:T(8,128)(2,1)}, u32[]{:S(2)}) copy-start(bf16[128,2048]{1,0:T(8,128)(2,1)} %param.19) | copy-start | bytes 1572868
Sparse Core Ops, SparseCore 0:
  51.8 118.3 all-gather.14
  173.1 112.7 all-gather.12
  288.8 141.6 all-gather.16
  433.2 142.0 all-gather.8
  578.0 142.0 all-gather.10
